TPU v7x, 32 devices: a whole 2x2x4 slice. The times are simulated.
32 devices in a mesh: sp: 8 (over z, x), tp: 4 (over y, core).
Axes of the slice: x: 2, y: 2, z: 4, core: 2. Of those that a mesh axis runs over, the one named last changes fastest.
Arguments:
- queries: bfloat16 [1024, 2048], P('sp', 'tp'), may hold values from -6 to 6
- key_rows: bfloat16 [1024, 2048], P('sp', 'tp'), may hold values from -6 to 6
- value_rows: bfloat16 [1024, 2048], P('sp', 'tp'), may hold values from -6 to 6
- gate_input: bfloat16 [1024, 2048], P('sp', 'tp'), may hold values from -6 to 6
- log_decay: float32 [1024, 16], P('sp', 'tp'), may hold values from -0.6 to 0, as said below
- head_gain: float32 [2048], P('tp'), may hold values from 0.1 to 1.9
- out_weight: bfloat16 [2048, 2048], P('tp'), may hold values from -0.125 to 0.125
- residual: bfloat16 [1024, 2048], P('sp'), may hold values from -6 to 6
- mlp_gain: float32 [2048], replicated, may hold values from 0.1 to 1.9
- gate_weight: bfloat16 [2048, 5632], P('sp', 'tp'), may hold values from -0.125 to 0.125
- up_weight: bfloat16 [2048, 5632], P('sp', 'tp'), may hold values from -0.125 to 0.125
- down_weight: bfloat16 [5632, 2048], P('tp', 'sp'), may hold values from -0.078125 to 0.078125
Outputs:
- layer_out: bfloat16 [1024, 2048], P(('sp', 'tp'))
Inputs may be any that keep to these rules, and one draw needn't show every extreme that they name: log_decay holds the logarithm of a decay factor of each head at each position.
All inputs are finite; a program needn't handle non-finite values.
Results may differ from a plain program's by a relative error of at most 0.017.
Values may be sent and summed in bfloat16 or wider, within the bound.
A program may use at most 128 MiB of HBM per device.

v0:
```python
import jax
import jax.numpy as jnp
from jax import lax
from jax.sharding import PartitionSpec as P

BLOCK = 128


EPS = 1e-06


def prefix_2(x, axis, join, neutral):
    place = lax.axis_index(axis)
    gathered = jax.tree.map(
        lambda a, kind: lax.all_gather(a.astype(kind), axis), x, (jnp.bfloat16, jnp.bfloat16)
    )
    state = jax.tree.map(lambda a, e: jnp.zeros_like(a) + jnp.asarray(e, a.dtype), x, neutral)

    def one(step, state):
        return join(
            state,
            jax.tree.map(
                lambda a, own: lax.dynamic_index_in_dim(a, step, 0, False).astype(own.dtype),
                gathered,
                x,
            ),
        )

    return lax.fori_loop(0, place, one, state)


def rotate(values_in, positions):
    half = values_in.shape[-1] // 2
    freq = 10000.0 ** (-jnp.linspace(0.0, 1.0, half, dtype=jnp.float32))
    angles = positions * freq
    angles = jnp.concatenate([angles, angles], axis=-1)
    first = values_in[..., :half]
    second = values_in[..., half:]
    turned = jnp.concatenate([-second, first], axis=-1)
    return values_in * jnp.cos(angles) + turned * jnp.sin(angles)


def row_norm(stream, gain):
    return stream * lax.rsqrt(jnp.mean(stream * stream, axis=-1, keepdims=True) + EPS) * gain


def join_states(earlier, later):
    return (earlier[0] * later[0], later[0][:, None, None] * earlier[1] + later[1])


def body(
    queries,
    key_rows,
    value_rows,
    gate_input,
    log_decay,
    head_gain,
    out_weight,
    residual,
    mlp_gain,
    gate_weight,
    up_weight,
    down_weight,
):
    tok_rows = queries.shape[0]
    heads_here = log_decay.shape[1]
    head_size = head_gain.shape[0] // heads_here
    quarter = tok_rows // lax.axis_size("tp")
    offset = lax.axis_index("sp") * tok_rows
    positions = (offset + lax.iota(jnp.int32, tok_rows)).astype(jnp.float32)[:, None, None]
    q_rot = rotate(
        queries.reshape(tok_rows, heads_here, head_size).astype(jnp.float32), positions
    ).astype(jnp.bfloat16)
    k_rot = (
        rotate(key_rows.reshape(tok_rows, heads_here, head_size).astype(jnp.float32), positions)
        * head_size ** (-0.5)
    ).astype(jnp.bfloat16)
    blocks = tok_rows // BLOCK
    q_blocks = q_rot.reshape(blocks, BLOCK, heads_here, head_size)
    k_blocks = k_rot.reshape(blocks, BLOCK, heads_here, head_size)
    v_blocks = value_rows.reshape(blocks, BLOCK, heads_here, head_size)
    cumul = jnp.cumsum(log_decay.reshape(blocks, BLOCK, heads_here), axis=1)
    by_head = cumul.transpose(0, 2, 1)
    lower = jnp.tril(jnp.ones((BLOCK, BLOCK), dtype=bool))
    spread = by_head[:, :, :, None] - by_head[:, :, None, :]
    weight = jnp.where(lower, jnp.exp(jnp.where(lower, spread, 0.0)), 0.0)
    scores = jnp.einsum("nthd,nshd->nhts", q_blocks, k_blocks, preferred_element_type=jnp.float32)
    probs = (scores * weight).astype(jnp.bfloat16)
    inner = jnp.einsum("nhts,nshe->nthe", probs, v_blocks, preferred_element_type=jnp.float32)
    k_weighted = (
        k_blocks.astype(jnp.float32) * jnp.exp(cumul[:, -1:, :] - cumul)[..., None]
    ).astype(jnp.bfloat16)
    contrib = jnp.einsum(
        "nshd,nshe->nhde", k_weighted, v_blocks, preferred_element_type=jnp.float32
    )
    totals = jnp.exp(cumul[:, -1, :])

    def advance(carry, items):
        state, prefix = carry
        factor, update = items
        return ((state * factor[:, None, None] + update, prefix * factor), (state, prefix))

    start_state = jnp.zeros((heads_here, head_size, head_size), jnp.float32)
    start_prefix = jnp.ones((heads_here,), jnp.float32)
    (dev_state, dev_total), (local_before, prefixes) = lax.scan(
        advance, (start_state, start_prefix), (totals, contrib)
    )
    _, incoming = prefix_2((dev_total, dev_state), "sp", join_states, (start_prefix, start_state))
    before = local_before + prefixes[:, :, None, None] * incoming[None]
    cross = jnp.einsum(
        "nthd,nhde->nthe", q_blocks.astype(jnp.float32), before, precision=lax.Precision.HIGHEST
    )
    cross = cross * jnp.exp(cumul)[..., None]
    result = (inner + cross).reshape(tok_rows, heads_here, head_size)
    result = row_norm(result, head_gain.reshape(heads_here, head_size)).reshape(
        tok_rows, heads_here * head_size
    )
    retained = (result * jax.nn.silu(gate_input.astype(jnp.float32))).astype(jnp.bfloat16)
    picked = retained
    mixed = lax.psum_scatter(
        jnp.dot(picked, out_weight, preferred_element_type=jnp.float32).astype(jnp.bfloat16),
        "tp",
        scatter_dimension=0,
        tiled=True,
    ).astype(jnp.float32)
    own_rows = lax.dynamic_slice_in_dim(residual, lax.axis_index("tp") * quarter, quarter, 0)
    rows_mid = (own_rows.astype(jnp.float32) + mixed).astype(jnp.bfloat16)
    own_normed = row_norm(rows_mid.astype(jnp.float32), mlp_gain).astype(jnp.bfloat16)
    normed = lax.all_gather(own_normed, "tp", axis=0, tiled=True)
    gate = jnp.dot(
        normed,
        lax.all_gather(gate_weight, "sp", axis=0, tiled=True),
        preferred_element_type=jnp.float32,
    )
    upvals = jnp.dot(
        normed,
        lax.all_gather(up_weight, "sp", axis=0, tiled=True),
        preferred_element_type=jnp.float32,
    )
    full_down = lax.all_gather(down_weight, "sp", axis=1, tiled=True)
    hidden = (jax.nn.silu(gate) * upvals).astype(jnp.bfloat16)
    picked = hidden
    ffn = lax.psum_scatter(
        jnp.dot(picked, full_down, preferred_element_type=jnp.float32).astype(jnp.bfloat16),
        "tp",
        scatter_dimension=0,
        tiled=True,
    ).astype(jnp.float32)
    return (rows_mid.astype(jnp.float32) + ffn).astype(jnp.bfloat16)


def solution(mesh):
    return jax.shard_map(
        body,
        mesh=mesh,
        in_specs=(
            P("sp", "tp"),
            P("sp", "tp"),
            P("sp", "tp"),
            P("sp", "tp"),
            P("sp", "tp"),
            P("tp"),
            P("tp", None),
            P("sp", None),
            P(),
            P("sp", "tp"),
            P("sp", "tp"),
            P("tp", "sp"),
        ),
        out_specs=P(("sp", "tp"), None),
        check_vma=False,
    )
```

profile of v0, /device:TPU:0, one launch (start us, length us, event | category | flops | bytes accessed | tf_op | source)
XLA Modules:
  0.0 402.8 jit_solution(3665025626243340659)
XLA Ops:
  6.5 0.0 copy-start
  6.5 0.0 copy-start.2
  6.5 0.0 all-gather.13.cloned.1.call-start
  6.6 1.0 copy.56
  7.5 0.2 reduce_window_sum.13
  7.7 0.1 copy.61
  7.8 1.0 copy_bitcast_fusion
  8.7 0.0 copy-start.3
  8.7 0.0 copy-start.4
  8.8 1.0 copy_bitcast_fusion.1
  9.7 0.1 fusion.40
  9.8 0.1 broadcast_multiply_fusion
  9.9 0.3 fusion.38
  10.2 0.2 slice_negate_fusion
  10.4 0.1 bitcast_exponential_fusion
  10.5 1.2 fusion.19
  11.7 1.9 fusion.4
  13.6 0.0 all-gather.13.cloned.1.call-update
  13.6 0.0 reduce-scatter.3.cloned.1.call-start
  13.7 22.3 %all-gather = bf16[8,1,4]{2,1,0:T(2,128)(2,1)S(1)} all-gather(bf16[1,1,4]{2,1,0:T(2,128)(2,1)S(1)} %get-tuple-element.106), channel_id=2, replica_groups=mesh['sp'=8,'tp'=4] {'sp'}, dimensions={0}, use_global_device_ids=true | all-gather | bytes 72 | tf_op jit(solution)/shard_map/all_gather | solution.py:15
  35.9 0.1 copy.57
  36.0 0.1 copy.60
  36.1 0.1 copy.64
  36.2 0.0 copy-done.2
  36.2 0.4 convolution_bitcast_fusion.1
  36.6 20.1 %all-gather.13.cloned.1.call-done = bf16[32,128,128]{2,1,0:T(8,128)(2,1)} async-done(((bf16[4,128,128]{2,1,0:T(8,128)(2,1)}), bf16[32,128,128]{2,1,0:T(8,128)(2,1)}) %all-gather.13.cloned.1.call-update) | async-done | bytes 1048592 | tf_op jit(solution)/shard_map/all_gather | solution.py:15
  56.8 0.0 copy-start.1
  56.8 0.4 multiply_reduce_fusion
  57.2 0.1 copy.66
  57.4 0.1 copy.67
  57.5 0.2 mul.242
  57.7 0.0 copy-done
  57.7 0.0 copy-done.3
  57.7 0.0 copy-done.4
  57.7 1.3 convolution_convert_fusion
  59.0 0.0 reduce-scatter.3.cloned.1.call-update
  59.0 0.0 all-gather.7.cloned.1.call-start
  59.1 0.7 all-gather.7.cloned.1.call-update
  59.8 0.0 all-gather.11.cloned.1.call-start
  59.8 0.5 all-gather.11.cloned.1.call-update
  60.3 0.0 all-gather.9.cloned.1.call-start
  60.4 0.5 all-gather.9.cloned.1.call-update
  60.9 0.0 reduce-scatter.5.cloned.1.call-start
  61.0 26.0 %reduce-scatter.3.cloned.1.call-done = bf16[32,2048]{1,0:T(8,128)(2,1)} async-done(((bf16[128,2048]{1,0:T(8,128)(2,1)}), bf16[32,2048]{1,0:T(8,128)(2,1)}) %reduce-scatter.3.cloned.1.call-update) | async-done | bytes 131088 | tf_op jit(solution)/shard_map/reduce_scatter | solution.py:120
  87.0 1.1 fusion.10
  88.1 0.0 copy-done.1
  88.1 0.1 fusion.12
  88.2 6.6 %all_gather.22 = bf16[128,2048]{1,0:T(8,128)(2,1)S(1)} all-gather(bf16[32,2048]{1,0:T(8,128)(2,1)S(1)} %fusion.12), channel_id=1, replica_groups=mesh['sp'=8,'tp'=4] {'tp'}, dimensions={0}, use_global_device_ids=true | all-gather | bytes 655360 | tf_op jit(solution)/shard_map/all_gather | solution.py:129
  94.8 86.7 %all-gather.7.cloned.1.call-done = bf16[2048,1408]{1,0:T(8,128)(2,1)} async-done(((bf16[256,1408]{1,0:T(8,128)(2,1)}), bf16[2048,1408]{1,0:T(8,128)(2,1)}) %all-gather.7.cloned.1.call-update) | async-done | bytes 5767184 | tf_op jit(solution)/shard_map/all_gather | solution.py:132
  181.5 3.6 fusion.44
  185.1 89.6 %all-gather.11.cloned.1.call-done = bf16[1408,2048]{1,0:T(8,128)(2,1)} async-done(((bf16[1408,256]{1,0:T(8,128)(2,1)}), bf16[1408,2048]{1,0:T(8,128)(2,1)}) %all-gather.11.cloned.1.call-update) | async-done | bytes 5767184 | tf_op jit(solution)/shard_map/all_gather | solution.py:140
  274.7 92.6 %all-gather.9.cloned.1.call-done = bf16[2048,1408]{1,0:T(8,128)(2,1)} async-done(((bf16[256,1408]{1,0:T(8,128)(2,1)}), bf16[2048,1408]{1,0:T(8,128)(2,1)}) %all-gather.9.cloned.1.call-update) | async-done | bytes 5767184 | tf_op jit(solution)/shard_map/all_gather | solution.py:137
  367.3 7.1 %convolution_convert_fusion.1 = bf16[128,2048]{1,0:T(8,128)(2,1)} fusion(bf16[1408,2048]{1,0:T(8,128)(2,1)} %all-gather.11.cloned.1.call-done, bf16[128,2048]{1,0:T(8,128)(2,1)S(1)} %all_gather.22, bf16[2048,1408]{1,0:T(8,128)(2,1)} %all-gather.9.cloned.1.call-done, f32[128,1408]{1,0:T(8,128)S(1)} %fusion.44), kind=kOutput, calls=%fused_computation.5 | convolution fusion | flops 1477738496 | bytes 13303808 | tf_op jit(solution)/shard_map/dot_general | solution.py:144
  374.4 0.0 reduce-scatter.5.cloned.1.call-update
  374.4 20.0 %reduce-scatter.5.cloned.1.call-done = bf16[32,2048]{1,0:T(8,128)(2,1)} async-done(((bf16[128,2048]{1,0:T(8,128)(2,1)}), bf16[32,2048]{1,0:T(8,128)(2,1)}) %reduce-scatter.5.cloned.1.call-update) | async-done | bytes 131088 | tf_op jit(solution)/shard_map/reduce_scatter | solution.py:143
  394.4 1.6 fusion.13
  (9 shorter events, 0.1 us)
Async XLA Ops:
  6.5 51.2 %copy-start = (bf16[512,2048]{1,0:T(8,128)(2,1)S(1)}, bf16[512,2048]{1,0:T(8,128)(2,1)}, u32[]{:S(2)}) copy-start(bf16[512,2048]{1,0:T(8,128)(2,1)} %param.22) | copy-start | bytes 6291460
  6.5 29.7 %copy-start.2 = (bf16[128,512]{1,0:T(8,128)(2,1)S(1)}, bf16[128,512]{1,0:T(8,128)(2,1)}, u32[]{:S(2)}) copy-start(bf16[128,512]{1,0:T(8,128)(2,1)} %param.18) | copy-start | bytes 393220
  6.5 50.2 %all-gather.13.cloned.1.call-start = ((), (), s32[]{:S(2)}) async-start(), calls=%async_computation.7 | async-start | bytes 1179648 | tf_op jit(solution)/shard_map/all_gather | solution.py:15
  8.7 49.0 %copy-start.3 = (bf16[128,512]{1,0:T(8,128)(2,1)S(1)}, bf16[128,512]{1,0:T(8,128)(2,1)}, u32[]{:S(2)}) copy-start(bf16[128,512]{1,0:T(8,128)(2,1)} %param.19) | copy-start | bytes 393220
  8.7 49.0 %copy-start.4 = (f32[512]{0:T(512)S(1)}, f32[512]{0:T(512)}, u32[]{:S(2)}) copy-start(f32[512]{0:T(512)} %param.21) | copy-start | bytes 6148
  13.6 73.4 %reduce-scatter.3.cloned.1.call-start = ((), (), s32[]{:S(2)}) async-start(), calls=%async_computation.2 | async-start | bytes 655360 | tf_op jit(solution)/shard_map/reduce_scatter | solution.py:120
  56.8 31.3 %copy-start.1 = (f32[2048]{0:T(1024)S(1)}, f32[2048]{0:T(1024)}, u32[]{:S(2)}) copy-start(f32[2048]{0:T(1024)} %param.24) | copy-start | bytes 24580
  59.0 122.5 %all-gather.7.cloned.1.call-start = ((), (), s32[]{:S(2)}) async-start(), calls=%async_computation.3 | async-start | bytes 6488064 | tf_op jit(solution)/shard_map/all_gather | solution.py:132
  59.8 215.0 %all-gather.11.cloned.1.call-start = ((), (), s32[]{:S(2)}) async-start(), calls=%async_computation.5 | async-start | bytes 6488064 | tf_op jit(solution)/shard_map/all_gather | solution.py:140
  60.3 306.9 %all-gather.9.cloned.1.call-start = ((), (), s32[]{:S(2)}) async-start(), calls=%async_computation.4 | async-start | bytes 6488064 | tf_op jit(solution)/shard_map/all_gather | solution.py:137
  60.9 333.5 %reduce-scatter.5.cloned.1.call-start = ((), (), s32[]{:S(2)}) async-start(), calls=%async_computation.6 | async-start | bytes 655360 | tf_op jit(solution)/shard_map/reduce_scatter | solution.py:143
Sparse Core Ops, SparseCore 0:
  13.7 42.9 all-gather.12
  59.3 27.6 reduce-scatter.2
  89.2 92.2 all-gather.6
  183.4 91.2 all-gather.10
  276.8 90.4 all-gather.8
  374.5 19.8 reduce-scatter.4
where the time goes:
time: 403 us
  waiting for transfers between devices  337 us (84%)
  blocking collectives  28.9 us (7%)
  matrix products  14.6 us (4%)
  between operations  13.6 us (3%)
  other arithmetic  6.89 us (2%)
    all_gather x1, waiting for transfers between devices, body(): lax.all_gather(up_weight, 'sp', axis=0, tiled=True)  92.6 us
    all_gather x1, waiting for transfers between devices, body(): full_down = lax.all_gather(down_weight, 'sp', axis=1, tiled=True)  89.6 us
    all_gather x1, waiting for transfers between devices, body(): lax.all_gather(gate_weight, 'sp', axis=0, tiled=True)  86.7 us
    reduce_scatter x1, waiting for transfers between devices, body(): lax.psum_scatter(jnp.dot(picked, out_weight, preferred_element_type=jnp.f...  26 us
    all_gather x1, blocking collectives, prefix_2(): lax.all_gather(a.astype(kind), axis)  22.3 us
    all_gather x1, waiting for transfers between devices, prefix_2(): lax.all_gather(a.astype(kind), axis)  20.1 us
    reduce_scatter x1, waiting for transfers between devices, body(): lax.psum_scatter(jnp.dot(picked, full_down, preferred_element_type=jnp.fl...  20 us
  transfers between devices with their start and end apart: 6, of which 6 were waited for; matrix products, arithmetic and copies ran while one was open for 1% of the time, Pallas kernels for 0%

commit v1 on v0

--- a/solution.py
+++ b/solution.py
@@ -1,6 +1,10 @@
+import functools
+
 import jax
 import jax.numpy as jnp
 from jax import lax
+from jax.experimental import pallas as pl
+from jax.experimental.pallas import tpu as pltpu
 from jax.sharding import PartitionSpec as P
 
 BLOCK = 128
@@ -149,24 +153,519 @@
     return (rows_mid.astype(jnp.float32) + ffn).astype(jnp.bfloat16)
 
 
+MESH = pl.DeviceIdType.MESH
+XS = 2
+CS = 2
+F32 = jnp.float32
+BF16 = jnp.bfloat16
+
+
+def dot_nt(a, b):
+    return lax.dot_general(a, b, (((1,), (1,)), ((), ())), preferred_element_type=F32)
+
+
+def dot_nn(a, b):
+    return lax.dot_general(a, b, (((1,), (0,)), ((), ())), preferred_element_type=F32)
+
+
+def kernel(
+    nz,
+    nt,
+    q_ref,
+    k_ref,
+    v_ref,
+    g_ref,
+    ld_ref,
+    cos_ref,
+    sin_ref,
+    hg_ref,
+    res_ref,
+    mg_ref,
+    ow_hbm,
+    gw_hbm,
+    uw_hbm,
+    dw_hbm,
+    out_ref,
+    ow,
+    w,
+    qrot,
+    inner,
+    cumx,
+    contrib,
+    c_out,
+    t_out,
+    c_in,
+    t_in,
+    p_out,
+    tt_out,
+    p_in,
+    tt_in,
+    retained,
+    mix_out,
+    mix_in,
+    middle,
+    norm_own,
+    normed,
+    keep,
+    s1,
+    r1,
+    s2,
+    r2,
+    s3,
+    r3,
+    ow_sem,
+    own_sem,
+    w_send,
+    w_recv,
+    f_send,
+    f_recv,
+    cx_send,
+    cx_recv,
+    pz_send,
+    pz_recv,
+    mix_send,
+    mix_recv,
+    nz_send,
+    nz_recv,
+    nt_send,
+    nt_recv,
+    t1_send,
+    t1_recv,
+    t2_send,
+    t2_recv,
+    t3_send,
+    t3_recv,
+):
+    sp = lax.axis_index("sp")
+    tp = lax.axis_index("tp")
+    z, x = sp // XS, lax.rem(sp, XS)
+    y, c = tp // CS, lax.rem(tp, CS)
+    rows = q_ref.shape[0]
+    heads = ld_ref.shape[1]
+    hd = q_ref.shape[1] // heads
+    quarter = rows // nt
+    weights = (gw_hbm, uw_hbm, dw_hbm)
+    x_peer = (z * XS + (1 - x), tp)
+    c_peer = (sp, y * CS + (1 - c))
+    y_peer = (sp, (1 - y) * CS + c)
+
+    def z_at(d):
+        return lax.rem(z + d, nz)
+
+    def z_peer(d):
+        return (z_at(d) * XS + x, tp)
+
+    def t_at(d):
+        return lax.rem(tp + d, nt)
+
+    def t_peer(d):
+        return (sp, t_at(d))
+
+    def remote(src, dst, send, recv, peer):
+        return pltpu.make_async_remote_copy(
+            src_ref=src,
+            dst_ref=dst,
+            send_sem=send,
+            recv_sem=recv,
+            device_id=peer,
+            device_id_type=MESH,
+        )
+
+    started = []
+
+    def go(copy):
+        copy.start()
+        started.append(copy)
+        return copy
+
+    ow_copy = pltpu.make_async_copy(ow_hbm, ow, ow_sem)
+    ow_copy.start()
+    own_copies = []
+    for m in range(3):
+        own = pltpu.make_async_copy(weights[m].at[z], w.at[m, sp], own_sem.at[m])
+        own.start()
+        own_copies.append(own)
+
+    barrier = pltpu.get_barrier_semaphore()
+    peers = [z_peer(d) for d in range(1, nz)] + [x_peer] + [t_peer(d) for d in range(1, nt)]
+    for peer in peers:
+        pl.semaphore_signal(barrier, inc=1, device_id=peer, device_id_type=MESH)
+    pl.semaphore_wait(barrier, len(peers))
+
+    w_copies = {}
+
+    def send_weight(m, d):
+        w_copies[m, d] = go(
+            remote(
+                weights[m].at[z_at(d)], w.at[m, sp], w_send.at[m, d], w_recv.at[m, d], z_peer(d)
+            )
+        )
+
+    f_copies = {}
+
+    def forward(m, d):
+        slot = lax.rem(z - d + nz, nz) * XS + x
+        if d == 0:
+            own_copies[m].wait()
+        else:
+            w_copies[m, d].wait_recv()
+        f_copies[m, d] = go(
+            remote(w.at[m, slot], w.at[m, slot], f_send.at[m, d], f_recv.at[m, d], x_peer)
+        )
+
+    send_weight(0, 2 % nz)
+
+    ti = lax.broadcasted_iota(jnp.int32, (rows, rows), 0)
+    si = lax.broadcasted_iota(jnp.int32, (rows, rows), 1)
+    lower = si <= ti
+    cumul = lax.dot_general(
+        lower.astype(F32),
+        ld_ref[...],
+        (((1,), (0,)), ((), ())),
+        precision=lax.Precision.HIGHEST,
+        preferred_element_type=F32,
+    )
+    cos, sin = cos_ref[...], sin_ref[...]
+    for h in range(heads):
+        cols = slice(h * hd, (h + 1) * hd)
+        qf = q_ref[:, cols].astype(F32)
+        kf = k_ref[:, cols].astype(F32)
+        vb = v_ref[:, cols]
+        qb = (qf * cos + pltpu.roll(qf, hd // 2, 1) * sin).astype(BF16)
+        kb = ((kf * cos + pltpu.roll(kf, hd // 2, 1) * sin) * hd ** (-0.5)).astype(BF16)
+        cum = jnp.broadcast_to(cumul[:, h : h + 1], (rows, rows))
+        spread = cum - jnp.transpose(cum)
+        weight = jnp.where(lower, jnp.exp(jnp.where(lower, spread, 0.0)), 0.0)
+        probs = (dot_nt(qb, kb) * weight).astype(BF16)
+        inner[:, cols] = dot_nn(probs, vb)
+        last = cum[rows - 1 :, :]
+        kw = kb.astype(F32) * jnp.exp(last - cum)
+        cb = dot_nn(jnp.transpose(kw).astype(BF16), vb)
+        contrib[h] = cb
+        c_out[h] = cb.astype(BF16)
+        t_out[h : h + 1, :] = jnp.exp(last)
+        qrot[:, cols] = qb.astype(F32)
+        cumx[:, cols] = jnp.exp(cum)
+    cx = go(remote(c_out, c_in, cx_send.at[0], cx_recv.at[0], x_peer))
+    tx = go(remote(t_out, t_in, cx_send.at[1], cx_recv.at[1], x_peer))
+    forward(0, 0)
+    cx.wait_recv()
+    tx.wait_recv()
+    first = x == 0
+    for h in range(heads):
+        own_c, own_t = contrib[h], t_out[h : h + 1, :]
+        other_c, other_t = c_in[h].astype(F32), t_in[h : h + 1, :]
+        plane = jnp.where(first, other_t * own_c + other_c, own_t * other_c + own_c)
+        p_out[h] = plane.astype(BF16)
+        tt_out[h : h + 1, :] = own_t * other_t
+    pz, tz = {}, {}
+    for d in range(1, nz):
+        pz[d] = go(remote(p_out, p_in.at[z], pz_send.at[0, d], pz_recv.at[0, d], z_peer(d)))
+        tz[d] = go(remote(tt_out, tt_in.at[z], pz_send.at[1, d], pz_recv.at[1, d], z_peer(d)))
+    for m in range(3):
+        for d in range(1, nz):
+            if (m, d) not in w_copies:
+                send_weight(m, d)
+    forward(1, 0)
+    forward(2, 0)
+    for d in range(1, nz):
+        pz[d].wait_recv()
+        tz[d].wait_recv()
+    p_in[z] = p_out[...]
+    tt_in[z] = tt_out[...]
+    for h in range(heads):
+        cols = slice(h * hd, (h + 1) * hd)
+        state = jnp.zeros((hd, hd), F32)
+        for zz in range(nz - 1):
+            later = tt_in[zz, h : h + 1, :] * state + p_in[zz, h].astype(F32)
+            state = jnp.where(zz < z, later, state)
+        state = jnp.where(first, state, t_in[h : h + 1, :] * state + c_in[h].astype(F32))
+        cross = lax.dot_general(
+            qrot[:, cols],
+            state,
+            (((1,), (0,)), ((), ())),
+            precision=lax.Precision.HIGHEST,
+            preferred_element_type=F32,
+        )
+        ret = inner[:, cols] + cumx[:, cols] * cross
+        scale = lax.rsqrt(jnp.mean(ret * ret, axis=-1, keepdims=True) + EPS)
+        gf = g_ref[:, cols].astype(F32)
+        retained[:, cols] = (
+            ret * scale * hg_ref[:, cols] * (gf / (1.0 + jnp.exp(-gf)))
+        ).astype(BF16)
+    ow_copy.wait()
+    for d in list(range(1, nt)) + [0]:
+        mine = pl.multiple_of(t_at(d) * quarter, quarter)
+        part = dot_nn(retained[pl.ds(mine, quarter), :], ow[...]).astype(BF16)
+        if d == 0:
+            mix_in[tp] = part
+        else:
+            mix_out[d] = part
+            go(
+                remote(
+                    mix_out.at[d], mix_in.at[tp], mix_send.at[d], mix_recv.at[d], t_peer(d)
+                )
+            )
+    for d in range(1, nt):
+        remote(
+            mix_out.at[d], mix_in.at[tp], mix_send.at[d], mix_recv.at[d], t_peer(d)
+        ).wait_recv()
+    mixed = mix_in[0].astype(F32)
+    for j in range(1, nt):
+        mixed += mix_in[j].astype(F32)
+    mine = pl.multiple_of(tp * quarter, quarter)
+    mid = (res_ref[pl.ds(mine, quarter), :].astype(F32) + mixed).astype(BF16).astype(F32)
+    middle[...] = mid
+    norm_own[...] = (
+        mid * lax.rsqrt(jnp.mean(mid * mid, axis=-1, keepdims=True) + EPS) * mg_ref[...]
+    ).astype(BF16)
+    normed[z, tp] = norm_own[...]
+    ncopy = {}
+    for d in range(1, nz):
+        ncopy[d] = go(
+            remote(norm_own, normed.at[z, tp], nz_send.at[d], nz_recv.at[d], z_peer(d))
+        )
+    tcopy = {}
+    for e in range(1, nt):
+        tcopy[0, e] = go(
+            remote(norm_own, normed.at[z, tp], nt_send.at[0, e], nt_recv.at[0, e], t_peer(e))
+        )
+    order = [2 % nz] + [d for d in range(1, nz) if d != 2 % nz]
+    for d in order:
+        forward(0, d)
+    for m in (1, 2):
+        for d in range(1, nz):
+            forward(m, d)
+    for d in range(1, nz):
+        ncopy[d].wait_recv()
+        zz = lax.rem(z - d + nz, nz)
+        for e in range(1, nt):
+            tcopy[d, e] = go(
+                remote(
+                    normed.at[zz, tp],
+                    normed.at[zz, tp],
+                    nt_send.at[d, e],
+                    nt_recv.at[d, e],
+                    t_peer(e),
+                )
+            )
+    for key in sorted(f_copies):
+        f_copies[key].wait_recv()
+    for key in sorted(tcopy):
+        tcopy[key].wait_recv()
+
+    ns = nz * XS
+    width = w.shape[3]
+    t1, t2 = {}, {}
+    chunks = [d for d in (2, 1, 3) if d < nz] + list(range(4, nz)) + [0]
+
+    def compute(d):
+        zz = z_at(d)
+        block = normed[zz].reshape(rows, normed.shape[3])
+        gate = dot_nt(block[:, :width], w[0, 0])
+        up = dot_nt(block[:, :width], w[1, 0])
+        for s in range(1, ns):
+            piece = block[:, s * width : (s + 1) * width]
+            gate += dot_nt(piece, w[0, s])
+            up += dot_nt(piece, w[1, s])
+        hidden = (gate / (1.0 + jnp.exp(-gate)) * up).astype(BF16)
+        low = c == 0
+        for s in range(ns):
+            part = dot_nn(hidden, w[2, s])
+            cols = slice(s * width, (s + 1) * width)
+            for yy in range(nt // CS):
+                even = part[(yy * CS) * quarter : (yy * CS + 1) * quarter]
+                odd = part[(yy * CS + 1) * quarter : (yy * CS + 2) * quarter]
+                keep[d, yy, :, cols] = jnp.where(low, even, odd)
+                s1[d, yy, :, cols] = jnp.where(low, odd, even).astype(BF16)
+        t1[d] = go(remote(s1.at[d], r1.at[d], t1_send.at[d], t1_recv.at[d], c_peer))
+
+    def second(d):
+        t1[d].wait_recv()
+        s2[d] = (keep[d, 1 - y] + r1[d, 1 - y].astype(F32)).astype(BF16)
+        t2[d] = go(remote(s2.at[d], r2.at[d], t2_send.at[d], t2_recv.at[d], y_peer))
+        keep[d, y] = keep[d, y] + r1[d, y].astype(F32)
+
+    t3 = {}
+
+    def third(d):
+        t2[d].wait_recv()
+        total = keep[d, y] + r2[d].astype(F32)
+        if d == 0:
+            middle[...] = middle[...] + total
+        else:
+            s3[d] = total.astype(BF16)
+            t3[d] = go(remote(s3.at[d], r3.at[d], t3_send.at[d], t3_recv.at[d], z_peer(d)))
+
+    count = len(chunks)
+    for step in range(count + 2):
+        if step < count:
+            compute(chunks[step])
+        if 1 <= step < count + 1:
+            second(chunks[step - 1])
+        if step >= 2:
+            third(chunks[step - 2])
+    total = middle[...]
+    for d in range(1, nz):
+        t3[d].wait_recv()
+        total += r3[d].astype(F32)
+    out_ref[...] = total.astype(BF16)
+    for copy in started:
+        copy.wait_send()
+
+
+def fast_body(
+    queries,
+    key_rows,
+    value_rows,
+    gate_input,
+    log_decay,
+    head_gain,
+    out_weight,
+    residual,
+    mlp_gain,
+    gate_weight,
+    up_weight,
+    down_weight,
+):
+    rows, wide = queries.shape
+    heads = log_decay.shape[1]
+    hd = wide // heads
+    model = residual.shape[1]
+    ns, nt = lax.axis_size("sp"), lax.axis_size("tp")
+    nz = ns // XS
+    quarter = rows // nt
+    width, units = gate_weight.shape
+    share = units // nz
+    offset = lax.axis_index("sp") * rows
+    positions = (offset + lax.iota(jnp.int32, rows)).astype(F32)[:, None]
+    half = hd // 2
+    freq = 10000.0 ** (-jnp.linspace(0.0, 1.0, half, dtype=F32))
+    angles = positions * freq
+    cos, sin = jnp.cos(angles), jnp.sin(angles)
+    cos = jnp.concatenate([cos, cos], axis=1)
+    sin = jnp.concatenate([-sin, sin], axis=1)
+    gw = gate_weight.T.reshape(nz, share, width)
+    uw = up_weight.T.reshape(nz, share, width)
+    dw = down_weight.reshape(nz, share, width)
+    vmem = pl.BlockSpec(memory_space=pltpu.VMEM)
+    anyspace = pl.BlockSpec(memory_space=pl.ANY)
+    dma = pltpu.SemaphoreType.DMA
+    scratch = [
+        pltpu.VMEM(out_weight.shape, BF16),
+        pltpu.VMEM((3, ns, share, width), BF16),
+        pltpu.VMEM((rows, wide), F32),
+        pltpu.VMEM((rows, wide), F32),
+        pltpu.VMEM((rows, wide), F32),
+        pltpu.VMEM((heads, hd, hd), F32),
+        pltpu.VMEM((heads, hd, hd), BF16),
+        pltpu.VMEM((heads, hd), F32),
+        pltpu.VMEM((heads, hd, hd), BF16),
+        pltpu.VMEM((heads, hd), F32),
+        pltpu.VMEM((heads, hd, hd), BF16),
+        pltpu.VMEM((heads, hd), F32),
+        pltpu.VMEM((nz, heads, hd, hd), BF16),
+        pltpu.VMEM((nz, heads, hd), F32),
+        pltpu.VMEM((rows, wide), BF16),
+        pltpu.VMEM((nt, quarter, model), BF16),
+        pltpu.VMEM((nt, quarter, model), BF16),
+        pltpu.VMEM((quarter, model), F32),
+        pltpu.VMEM((quarter, model), BF16),
+        pltpu.VMEM((nz, nt, quarter, model), BF16),
+        pltpu.VMEM((nz, nt // CS, quarter, model), F32),
+        pltpu.VMEM((nz, nt // CS, quarter, model), BF16),
+        pltpu.VMEM((nz, nt // CS, quarter, model), BF16),
+        pltpu.VMEM((nz, quarter, model), BF16),
+        pltpu.VMEM((nz, quarter, model), BF16),
+        pltpu.VMEM((nz, quarter, model), BF16),
+        pltpu.VMEM((nz, quarter, model), BF16),
+        dma,
+        dma((3,)),
+        dma((3, nz)),
+        dma((3, nz)),
+        dma((3, nz)),
+        dma((3, nz)),
+        dma((2,)),
+        dma((2,)),
+        dma((2, nz)),
+        dma((2, nz)),
+        dma((nt,)),
+        dma((nt,)),
+        dma((nz,)),
+        dma((nz,)),
+        dma((nz, nt)),
+        dma((nz, nt)),
+        dma((nz,)),
+        dma((nz,)),
+        dma((nz,)),
+        dma((nz,)),
+        dma((nz,)),
+        dma((nz,)),
+    ]
+    return pl.pallas_call(
+        functools.partial(kernel, nz, nt),
+        out_shape=jax.ShapeDtypeStruct((quarter, model), BF16),
+        in_specs=[vmem] * 10 + [anyspace] * 4,
+        out_specs=vmem,
+        scratch_shapes=scratch,
+        compiler_params=pltpu.CompilerParams(
+            collective_id=0, has_side_effects=True, vmem_limit_bytes=60 * 1024 * 1024
+        ),
+    )(
+        queries,
+        key_rows,
+        value_rows,
+        gate_input,
+        log_decay,
+        cos,
+        sin,
+        head_gain.reshape(1, wide),
+        residual,
+        mlp_gain.reshape(1, model),
+        out_weight,
+        gw,
+        uw,
+        dw,
+    )
+
+
+def fits(mesh, queries, log_decay, gate_weight):
+    ns, nt = mesh.shape["sp"], mesh.shape["tp"]
+    tokens, wide = queries.shape
+    if ns % XS or ns // XS < 3 or nt != 2 * CS or tokens // ns != BLOCK:
+        return False
+    nz = ns // XS
+    hidden = gate_weight.shape[1] // nt
+    return (
+        gate_weight.shape[0] // ns % 128 == 0
+        and hidden % (16 * nz) == 0
+        and wide // log_decay.shape[1] == 128
+        and BLOCK % (16 * nt) == 0
+    )
+
+
 def solution(mesh):
-    return jax.shard_map(
-        body,
-        mesh=mesh,
-        in_specs=(
-            P("sp", "tp"),
-            P("sp", "tp"),
-            P("sp", "tp"),
-            P("sp", "tp"),
-            P("sp", "tp"),
-            P("tp"),
-            P("tp", None),
-            P("sp", None),
-            P(),
-            P("sp", "tp"),
-            P("sp", "tp"),
-            P("tp", "sp"),
-        ),
-        out_specs=P(("sp", "tp"), None),
-        check_vma=False,
-    )
+    def run(*args):
+        good = fits(mesh, args[0], args[4], args[9])
+        return jax.shard_map(
+            fast_body if good else body,
+            mesh=mesh,
+            in_specs=(
+                P("sp", "tp"),
+                P("sp", "tp"),
+                P("sp", "tp"),
+                P("sp", "tp"),
+                P("sp", "tp"),
+                P("tp"),
+                P("tp", None),
+                P("sp", None),
+                P(),
+                P("sp", "tp"),
+                P("sp", "tp"),
+                P("tp", "sp"),
+            ),
+            out_specs=P(("sp", "tp"), None),
+            check_vma=False,
+        )(*args)
+
+    return run

time: 403 us -> 121 us (0.30)
  waiting for transfers between devices: 337 us -> 0 us
  Pallas kernels: 0 us -> 113 us
  blocking collectives: 28.9 us -> 0 us
  matrix products: 14.6 us -> 0 us
  between operations: 13.6 us -> 0.02 us
  other arithmetic: 6.89 us -> 1.16 us
  local copies, waits for them, and re-layouts: 1.78 us -> 6.45 us
    all_gather x4 -> x0, waiting for transfers between devices: 289 us -> none  [the longest x1 92.6 us: body(): lax.all_gather(up_weight, 'sp', axis=0, tiled=True)]
    pallas_call x0 -> x1, Pallas kernels: none -> 113 us  [fast_body(): pl.pallas_call(functools.partial(kernel, nz, nt), out_shape=jax.ShapeDtyp...]
    reduce_scatter x2 -> x0, waiting for transfers between devices: 46 us -> none  [the longest x1 26 us: body(): lax.psum_scatter(jnp.dot(picked, out_weight, preferred_element_type=jnp.f...]
    all_gather x2 -> x0, blocking collectives: 28.9 us -> none  [the longest x1 22.3 us: prefix_2(): lax.all_gather(a.astype(kind), axis)]
    dot_general x6 -> x0, matrix products: 14.6 us -> none  [the longest x1 7.07 us: body(): jnp.dot(picked, full_down, preferred_element_type=jnp.float32)]
    convert_element_type x6 -> x1, other arithmetic: 4.79 us -> 0.01 us  [fast_body(): positions = (offset + lax.iota(jnp.int32, rows)).astype(F32)[:, None]]
  transfers between devices with their start and end apart: 6 -> 0, of which waited for: 6 -> 0; matrix products, arithmetic and copies ran while one was open for 1% -> 0% of each run, Pallas kernels for 0% -> 0%
where the time goes in v1:
time: 121 us
  Pallas kernels  113 us (93%)
  local copies, waits for them, and re-layouts  6.45 us (5%)
    pallas_call x1, Pallas kernels, fast_body(): pl.pallas_call(functools.partial(kernel, nz, nt), out_shape=jax.ShapeDtyp...  113 us
    unnamed x4, local copies, waits for them, and re-layouts  3.05 us

profile of v1, /device:TPU:0, one launch (start us, length us, event | category | flops | bytes accessed | tf_op | source)
XLA Modules:
  0.0 120.6 jit_solution(15415062219013655448)
XLA Ops:
  0.0 0.0 copy-start
  0.0 0.1 fusion.1
  0.1 1.5 %copy.15.ld_ref = f32[128,4]{1,0:T(8,128)} copy(f32[128,4]{0,1:T(4,128)} %param.16) | data formatting | bytes 4096 | tf_op args[4]
  1.6 0.3 fusion
  1.9 0.8 pad_maximum_fusion
  2.7 2.2 %copy.13 = bf16[1408,256]{1,0:T(8,128)(2,1)} copy(bf16[1408,256]{0,1:T(8,128)(2,1)} %bitcast.10) | data formatting | bytes 1441792 | tf_op jit(solution)/shard_map/transpose | solution.py:548
  4.9 0.0 copy-done
  4.9 1.2 copy.14
  6.1 112.9 %shard_map.118 = bf16[32,2048]{1,0:T(8,128)(2,1)} custom-call(bf16[128,512]{1,0:T(8,128)(2,1)} %q_ref.1, bf16[128,512]{1,0:T(8,128)(2,1)} %k_ref.1, bf16[128,512]{1,0:T(8,128)(2,1)} %v_ref.1, bf16[128,512]{1,0:T(8,128)(2,1)} %g_ref.1, f32[128,4]{1,0:T(8,128)} %copy.15.ld_ref, f32[128,128]{1,0:T(8,128)} %get-tuple-element.8.cos_ref, ...), custom_call_target="tpu_custom_call" | custom-call | tf_op jit(solution)/shard_map/pallas_call | solution.py:605
  119.0 1.6 %copy.17 = bf16[32,2048]{1,0:T(8,128)(2,1)} copy(bf16[32,2048]{1,0:T(8,128)(2,1)} %shard_map.118) | data formatting | bytes 262144
  (2 shorter events, 0.0 us)
Async XLA Ops:
  0.0 4.9 %copy-start = (bf16[256,1408]{1,0:T(8,128)(2,1)S(1)}, bf16[256,1408]{1,0:T(8,128)(2,1)}, u32[]{:S(2)}) copy-start(bf16[256,1408]{1,0:T(8,128)(2,1)} %param.22) | copy-start | bytes 2162692

commit v2 on v1

--- a/solution.py
+++ b/solution.py
@@ -1,4 +1,5 @@
 import functools
+import math
 
 import jax
 import jax.numpy as jnp
@@ -176,8 +177,6 @@
     v_ref,
     g_ref,
     ld_ref,
-    cos_ref,
-    sin_ref,
     hg_ref,
     res_ref,
     mg_ref,
@@ -187,6 +186,8 @@
     dw_hbm,
     out_ref,
     ow,
+    raw,
+    turned,
     w,
     qrot,
     inner,
@@ -200,12 +201,16 @@
     tt_out,
     p_in,
     tt_in,
+    s_own,
+    s_out,
+    s_in,
     retained,
     mix_out,
     mix_in,
-    middle,
+    acc,
     norm_own,
     normed,
+    hidden,
     keep,
     s1,
     r1,
@@ -214,6 +219,7 @@
     s3,
     r3,
     ow_sem,
+    raw_sem,
     own_sem,
     w_send,
     w_recv,
@@ -223,6 +229,8 @@
     cx_recv,
     pz_send,
     pz_recv,
+    sx_send,
+    sx_recv,
     mix_send,
     mix_recv,
     nz_send,
@@ -241,16 +249,21 @@
     z, x = sp // XS, lax.rem(sp, XS)
     y, c = tp // CS, lax.rem(tp, CS)
     rows = q_ref.shape[0]
-    heads = ld_ref.shape[1]
+    heads = ld_ref.shape[0]
+    hh = heads // XS
     hd = q_ref.shape[1] // heads
     quarter = rows // nt
-    weights = (gw_hbm, uw_hbm, dw_hbm)
+    share, width = w.shape[2], w.shape[3]
+    group = XS * width
     x_peer = (z * XS + (1 - x), tp)
     c_peer = (sp, y * CS + (1 - c))
     y_peer = (sp, (1 - y) * CS + c)
 
     def z_at(d):
         return lax.rem(z + d, nz)
+
+    def z_from(d):
+        return lax.rem(z - d + nz, nz)
 
     def z_peer(d):
         return (z_at(d) * XS + x, tp)
@@ -278,13 +291,24 @@
         started.append(copy)
         return copy
 
+    def piece(m, zz):
+        at = pl.ds(pl.multiple_of(zz * share, 16), share)
+        return dw_hbm.at[at] if m == 2 else turned.at[m, at]
+
+    raw_copies = []
+    for m, source in enumerate((gw_hbm, uw_hbm)):
+        raw_copy = pltpu.make_async_copy(source, raw.at[m], raw_sem.at[m])
+        raw_copy.start()
+        raw_copies.append(raw_copy)
     ow_copy = pltpu.make_async_copy(ow_hbm, ow, ow_sem)
+    own_copies = {}
+
+    def take_own(m):
+        own_copies[m] = pltpu.make_async_copy(piece(m, z), w.at[m, sp], own_sem.at[m])
+        own_copies[m].start()
+
+    take_own(2)
     ow_copy.start()
-    own_copies = []
-    for m in range(3):
-        own = pltpu.make_async_copy(weights[m].at[z], w.at[m, sp], own_sem.at[m])
-        own.start()
-        own_copies.append(own)
 
     barrier = pltpu.get_barrier_semaphore()
     peers = [z_peer(d) for d in range(1, nz)] + [x_peer] + [t_peer(d) for d in range(1, nt)]
@@ -296,15 +320,13 @@
 
     def send_weight(m, d):
         w_copies[m, d] = go(
-            remote(
-                weights[m].at[z_at(d)], w.at[m, sp], w_send.at[m, d], w_recv.at[m, d], z_peer(d)
-            )
+            remote(piece(m, z_at(d)), w.at[m, sp], w_send.at[m, d], w_recv.at[m, d], z_peer(d))
         )
 
     f_copies = {}
 
     def forward(m, d):
-        slot = lax.rem(z - d + nz, nz) * XS + x
+        slot = z_from(d) * XS + x
         if d == 0:
             own_copies[m].wait()
         else:
@@ -313,28 +335,39 @@
             remote(w.at[m, slot], w.at[m, slot], f_send.at[m, d], f_recv.at[m, d], x_peer)
         )
 
-    send_weight(0, 2 % nz)
+    far = 2
+    near = [d for d in range(1, nz) if d != far]
+    send_weight(2, far)
 
     ti = lax.broadcasted_iota(jnp.int32, (rows, rows), 0)
     si = lax.broadcasted_iota(jnp.int32, (rows, rows), 1)
     lower = si <= ti
     cumul = lax.dot_general(
-        lower.astype(F32),
         ld_ref[...],
+        (ti <= si).astype(F32),
         (((1,), (0,)), ((), ())),
         precision=lax.Precision.HIGHEST,
         preferred_element_type=F32,
     )
-    cos, sin = cos_ref[...], sin_ref[...]
+    half = hd // 2
+    lane = lax.broadcasted_iota(jnp.int32, (1, hd), 1)
+    low_half = lane < half
+    index = jnp.where(low_half, lane, lane - half).astype(F32)
+    freq = jnp.exp(index * (-math.log(10000.0) / (half - 1)))
+    angles = (sp * rows + lax.broadcasted_iota(jnp.int32, (rows, hd), 0)).astype(F32) * freq
+    cos = jnp.cos(angles)
+    sin = jnp.sin(angles)
+    sin = jnp.where(low_half, -sin, sin)
     for h in range(heads):
         cols = slice(h * hd, (h + 1) * hd)
         qf = q_ref[:, cols].astype(F32)
         kf = k_ref[:, cols].astype(F32)
         vb = v_ref[:, cols]
-        qb = (qf * cos + pltpu.roll(qf, hd // 2, 1) * sin).astype(BF16)
-        kb = ((kf * cos + pltpu.roll(kf, hd // 2, 1) * sin) * hd ** (-0.5)).astype(BF16)
-        cum = jnp.broadcast_to(cumul[:, h : h + 1], (rows, rows))
-        spread = cum - jnp.transpose(cum)
+        qb = (qf * cos + pltpu.roll(qf, half, 1) * sin).astype(BF16)
+        kb = ((kf * cos + pltpu.roll(kf, half, 1) * sin) * hd ** (-0.5)).astype(BF16)
+        along = jnp.broadcast_to(cumul[h : h + 1, :], (rows, rows))
+        cum = jnp.transpose(along)
+        spread = cum - along
         weight = jnp.where(lower, jnp.exp(jnp.where(lower, spread, 0.0)), 0.0)
         probs = (dot_nt(qb, kb) * weight).astype(BF16)
         inner[:, cols] = dot_nn(probs, vb)
@@ -343,43 +376,57 @@
         cb = dot_nn(jnp.transpose(kw).astype(BF16), vb)
         contrib[h] = cb
         c_out[h] = cb.astype(BF16)
-        t_out[h : h + 1, :] = jnp.exp(last)
+        t_out[h] = jnp.broadcast_to(jnp.exp(last), t_out.shape[1:])
         qrot[:, cols] = qb.astype(F32)
         cumx[:, cols] = jnp.exp(cum)
-    cx = go(remote(c_out, c_in, cx_send.at[0], cx_recv.at[0], x_peer))
+    mine_h, other_h = x * hh, (1 - x) * hh
+    cx = go(remote(c_out.at[pl.ds(other_h, hh)], c_in, cx_send.at[0], cx_recv.at[0], x_peer))
     tx = go(remote(t_out, t_in, cx_send.at[1], cx_recv.at[1], x_peer))
-    forward(0, 0)
+    forward(2, 0)
+    for m in range(2):
+        raw_copies[m].wait()
+        for j in range(raw.shape[2] // 128):
+            turned[m, j * 128 : (j + 1) * 128, :] = jnp.transpose(
+                raw[m, :, j * 128 : (j + 1) * 128]
+            )
+        take_own(m)
     cx.wait_recv()
     tx.wait_recv()
     first = x == 0
-    for h in range(heads):
-        own_c, own_t = contrib[h], t_out[h : h + 1, :]
-        other_c, other_t = c_in[h].astype(F32), t_in[h : h + 1, :]
+    for i in range(hh):
+        own_c, own_t = contrib[mine_h + i], t_out[mine_h + i][:1]
+        other_c, other_t = c_in[i].astype(F32), t_in[mine_h + i][:1]
         plane = jnp.where(first, other_t * own_c + other_c, own_t * other_c + own_c)
-        p_out[h] = plane.astype(BF16)
-        tt_out[h : h + 1, :] = own_t * other_t
+        p_out[i] = plane.astype(BF16)
+        tt_out[i] = jnp.broadcast_to(own_t * other_t, tt_out.shape[1:])
     pz, tz = {}, {}
     for d in range(1, nz):
         pz[d] = go(remote(p_out, p_in.at[z], pz_send.at[0, d], pz_recv.at[0, d], z_peer(d)))
         tz[d] = go(remote(tt_out, tt_in.at[z], pz_send.at[1, d], pz_recv.at[1, d], z_peer(d)))
-    for m in range(3):
-        for d in range(1, nz):
-            if (m, d) not in w_copies:
-                send_weight(m, d)
-    forward(1, 0)
-    forward(2, 0)
+    for d in [far] + near:
+        send_weight(0, d)
+    send_weight(1, far)
+    forward(0, 0)
     for d in range(1, nz):
         pz[d].wait_recv()
         tz[d].wait_recv()
     p_in[z] = p_out[...]
     tt_in[z] = tt_out[...]
-    for h in range(heads):
-        cols = slice(h * hd, (h + 1) * hd)
+    for i in range(hh):
         state = jnp.zeros((hd, hd), F32)
         for zz in range(nz - 1):
-            later = tt_in[zz, h : h + 1, :] * state + p_in[zz, h].astype(F32)
+            later = tt_in[zz, i][:1] * state + p_in[zz, i].astype(F32)
             state = jnp.where(zz < z, later, state)
-        state = jnp.where(first, state, t_in[h : h + 1, :] * state + c_in[h].astype(F32))
+        early_t = jnp.where(first, t_out[mine_h + i][:1], t_in[mine_h + i][:1])
+        early_c = jnp.where(first, contrib[mine_h + i], c_in[i].astype(F32))
+        after = early_t * state + early_c
+        s_own[i] = jnp.where(first, state, after)
+        s_out[i] = jnp.where(first, after, state).astype(BF16)
+    sx = go(remote(s_out, s_in, sx_send, sx_recv, x_peer))
+    forward(1, 0)
+    forward(2, far)
+
+    def finish(h, state, cols):
         cross = lax.dot_general(
             qrot[:, cols],
             state,
@@ -393,7 +440,15 @@
         retained[:, cols] = (
             ret * scale * hg_ref[:, cols] * (gf / (1.0 + jnp.exp(-gf)))
         ).astype(BF16)
+
+    sx.wait_recv()
+    for h in range(heads):
+        cols = slice(h * hd, (h + 1) * hd)
+        i = h % hh
+        mine = x == h // hh
+        finish(h, jnp.where(mine, s_own[i], s_in[i].astype(F32)), cols)
     ow_copy.wait()
+    mixes = []
     for d in list(range(1, nt)) + [0]:
         mine = pl.multiple_of(t_at(d) * quarter, quarter)
         part = dot_nn(retained[pl.ds(mine, quarter), :], ow[...]).astype(BF16)
@@ -401,44 +456,46 @@
             mix_in[tp] = part
         else:
             mix_out[d] = part
-            go(
-                remote(
-                    mix_out.at[d], mix_in.at[tp], mix_send.at[d], mix_recv.at[d], t_peer(d)
+            mixes.append(
+                go(
+                    remote(
+                        mix_out.at[d], mix_in.at[tp], mix_send.at[d], mix_recv.at[d], t_peer(d)
+                    )
                 )
             )
-    for d in range(1, nt):
-        remote(
-            mix_out.at[d], mix_in.at[tp], mix_send.at[d], mix_recv.at[d], t_peer(d)
-        ).wait_recv()
+    forward(0, far)
+    for mix in mixes:
+        mix.wait_recv()
     mixed = mix_in[0].astype(F32)
     for j in range(1, nt):
         mixed += mix_in[j].astype(F32)
     mine = pl.multiple_of(tp * quarter, quarter)
     mid = (res_ref[pl.ds(mine, quarter), :].astype(F32) + mixed).astype(BF16).astype(F32)
-    middle[...] = mid
+    for g in range(nz):
+        acc[g] = mid[:, g * group : (g + 1) * group]
     norm_own[...] = (
         mid * lax.rsqrt(jnp.mean(mid * mid, axis=-1, keepdims=True) + EPS) * mg_ref[...]
     ).astype(BF16)
     normed[z, tp] = norm_own[...]
-    ncopy = {}
-    for d in range(1, nz):
+    ncopy, tcopy = {}, {}
+    for d in [far] + near:
         ncopy[d] = go(
             remote(norm_own, normed.at[z, tp], nz_send.at[d], nz_recv.at[d], z_peer(d))
         )
-    tcopy = {}
     for e in range(1, nt):
         tcopy[0, e] = go(
             remote(norm_own, normed.at[z, tp], nt_send.at[0, e], nt_recv.at[0, e], t_peer(e))
         )
-    order = [2 % nz] + [d for d in range(1, nz) if d != 2 % nz]
-    for d in order:
+    for d in near:
+        send_weight(1, d)
+    for d in near:
+        send_weight(2, d)
+    for d in near:
         forward(0, d)
-    for m in (1, 2):
-        for d in range(1, nz):
-            forward(m, d)
-    for d in range(1, nz):
+    forward(1, far)
+    for d in [far] + near:
         ncopy[d].wait_recv()
-        zz = lax.rem(z - d + nz, nz)
+        zz = z_from(d)
         for e in range(1, nt):
             tcopy[d, e] = go(
                 remote(
@@ -449,67 +506,79 @@
                     t_peer(e),
                 )
             )
-    for key in sorted(f_copies):
-        f_copies[key].wait_recv()
+    for d in near:
+        forward(1, d)
+    for d in range(nz):
+        f_copies[0, d].wait_recv()
+        f_copies[1, d].wait_recv()
     for key in sorted(tcopy):
         tcopy[key].wait_recv()
 
     ns = nz * XS
-    width = w.shape[3]
-    t1, t2 = {}, {}
-    chunks = [d for d in (2, 1, 3) if d < nz] + list(range(4, nz)) + [0]
-
-    def compute(d):
-        zz = z_at(d)
+    for zz in range(nz):
         block = normed[zz].reshape(rows, normed.shape[3])
         gate = dot_nt(block[:, :width], w[0, 0])
         up = dot_nt(block[:, :width], w[1, 0])
         for s in range(1, ns):
-            piece = block[:, s * width : (s + 1) * width]
-            gate += dot_nt(piece, w[0, s])
-            up += dot_nt(piece, w[1, s])
-        hidden = (gate / (1.0 + jnp.exp(-gate)) * up).astype(BF16)
-        low = c == 0
-        for s in range(ns):
-            part = dot_nn(hidden, w[2, s])
-            cols = slice(s * width, (s + 1) * width)
-            for yy in range(nt // CS):
-                even = part[(yy * CS) * quarter : (yy * CS + 1) * quarter]
-                odd = part[(yy * CS + 1) * quarter : (yy * CS + 2) * quarter]
-                keep[d, yy, :, cols] = jnp.where(low, even, odd)
-                s1[d, yy, :, cols] = jnp.where(low, odd, even).astype(BF16)
-        t1[d] = go(remote(s1.at[d], r1.at[d], t1_send.at[d], t1_recv.at[d], c_peer))
-
-    def second(d):
-        t1[d].wait_recv()
-        s2[d] = (keep[d, 1 - y] + r1[d, 1 - y].astype(F32)).astype(BF16)
-        t2[d] = go(remote(s2.at[d], r2.at[d], t2_send.at[d], t2_recv.at[d], y_peer))
-        keep[d, y] = keep[d, y] + r1[d, y].astype(F32)
-
-    t3 = {}
-
-    def third(d):
-        t2[d].wait_recv()
-        total = keep[d, y] + r2[d].astype(F32)
-        if d == 0:
-            middle[...] = middle[...] + total
-        else:
-            s3[d] = total.astype(BF16)
-            t3[d] = go(remote(s3.at[d], r3.at[d], t3_send.at[d], t3_recv.at[d], z_peer(d)))
-
-    count = len(chunks)
+            cut = block[:, s * width : (s + 1) * width]
+            gate += dot_nt(cut, w[0, s])
+            up += dot_nt(cut, w[1, s])
+        hidden[zz * rows : (zz + 1) * rows, :] = (
+            gate / (1.0 + jnp.exp(-gate)) * up
+        ).astype(BF16)
+
+    t1, t2, t3 = {}, {}, {}
+    low = c == 0
+
+    def compute(b):
+        if b in near:
+            forward(2, b)
+        f_copies[2, b].wait_recv()
+        for u in range(XS):
+            part = dot_nn(hidden[...], w[2, z_from(b) * XS + u])
+            cols = slice(u * width, (u + 1) * width)
+            for zz in range(nz):
+                for yy in range(nt // CS):
+                    at = zz * rows + yy * CS * quarter
+                    even = part[at : at + quarter]
+                    odd = part[at + quarter : at + 2 * quarter]
+                    keep[b, yy, zz, :, cols] = jnp.where(low, even, odd)
+                    s1[b, yy, zz, :, cols] = jnp.where(low, odd, even).astype(BF16)
+        t1[b] = go(remote(s1.at[b], r1.at[b], t1_send.at[b], t1_recv.at[b], c_peer))
+
+    def second(b):
+        t1[b].wait_recv()
+        s2[b] = (keep[b, 1 - y] + r1[b, 1 - y].astype(F32)).astype(BF16)
+        t2[b] = go(remote(s2.at[b], r2.at[b], t2_send.at[b], t2_recv.at[b], y_peer))
+        keep[b, y] = keep[b, y] + r1[b, y].astype(F32)
+
+    def third(b):
+        t2[b].wait_recv()
+        for e in [far] + near:
+            zz = z_at(e)
+            s3[b, e] = (keep[b, y, zz] + r2[b, zz].astype(F32)).astype(BF16)
+            t3[b, e] = go(
+                remote(s3.at[b, e], r3.at[b, e], t3_send.at[b, e], t3_recv.at[b, e], z_peer(e))
+            )
+        g = z_from(b)
+        acc[g] = acc[g] + keep[b, y, z] + r2[b, z].astype(F32)
+
+    batches = [0, far] + near
+    count = len(batches)
     for step in range(count + 2):
         if step < count:
-            compute(chunks[step])
+            compute(batches[step])
         if 1 <= step < count + 1:
-            second(chunks[step - 1])
+            second(batches[step - 1])
         if step >= 2:
-            third(chunks[step - 2])
-    total = middle[...]
-    for d in range(1, nz):
-        t3[d].wait_recv()
-        total += r3[d].astype(F32)
-    out_ref[...] = total.astype(BF16)
+            third(batches[step - 2])
+    for b in batches:
+        for e in [far] + near:
+            t3[b, e].wait_recv()
+            g = lax.rem(z - e - b + 2 * nz, nz)
+            acc[g] = acc[g] + r3[b, e].astype(F32)
+    for g in range(nz):
+        out_ref[:, g * group : (g + 1) * group] = acc[g].astype(BF16)
     for copy in started:
         copy.wait_send()
 
@@ -537,49 +606,47 @@
     quarter = rows // nt
     width, units = gate_weight.shape
     share = units // nz
-    offset = lax.axis_index("sp") * rows
-    positions = (offset + lax.iota(jnp.int32, rows)).astype(F32)[:, None]
-    half = hd // 2
-    freq = 10000.0 ** (-jnp.linspace(0.0, 1.0, half, dtype=F32))
-    angles = positions * freq
-    cos, sin = jnp.cos(angles), jnp.sin(angles)
-    cos = jnp.concatenate([cos, cos], axis=1)
-    sin = jnp.concatenate([-sin, sin], axis=1)
-    gw = gate_weight.T.reshape(nz, share, width)
-    uw = up_weight.T.reshape(nz, share, width)
-    dw = down_weight.reshape(nz, share, width)
+    group = XS * width
+    hh = heads // XS
     vmem = pl.BlockSpec(memory_space=pltpu.VMEM)
     anyspace = pl.BlockSpec(memory_space=pl.ANY)
     dma = pltpu.SemaphoreType.DMA
     scratch = [
         pltpu.VMEM(out_weight.shape, BF16),
+        pltpu.VMEM((2, width, units), BF16),
+        pltpu.VMEM((2, units, width), BF16),
         pltpu.VMEM((3, ns, share, width), BF16),
         pltpu.VMEM((rows, wide), F32),
         pltpu.VMEM((rows, wide), F32),
         pltpu.VMEM((rows, wide), F32),
         pltpu.VMEM((heads, hd, hd), F32),
         pltpu.VMEM((heads, hd, hd), BF16),
-        pltpu.VMEM((heads, hd), F32),
-        pltpu.VMEM((heads, hd, hd), BF16),
-        pltpu.VMEM((heads, hd), F32),
-        pltpu.VMEM((heads, hd, hd), BF16),
-        pltpu.VMEM((heads, hd), F32),
-        pltpu.VMEM((nz, heads, hd, hd), BF16),
-        pltpu.VMEM((nz, heads, hd), F32),
+        pltpu.VMEM((heads, 8, hd), F32),
+        pltpu.VMEM((hh, hd, hd), BF16),
+        pltpu.VMEM((heads, 8, hd), F32),
+        pltpu.VMEM((hh, hd, hd), BF16),
+        pltpu.VMEM((hh, 8, hd), F32),
+        pltpu.VMEM((nz, hh, hd, hd), BF16),
+        pltpu.VMEM((nz, hh, 8, hd), F32),
+        pltpu.VMEM((hh, hd, hd), F32),
+        pltpu.VMEM((hh, hd, hd), BF16),
+        pltpu.VMEM((hh, hd, hd), BF16),
         pltpu.VMEM((rows, wide), BF16),
         pltpu.VMEM((nt, quarter, model), BF16),
         pltpu.VMEM((nt, quarter, model), BF16),
-        pltpu.VMEM((quarter, model), F32),
+        pltpu.VMEM((nz, quarter, group), F32),
         pltpu.VMEM((quarter, model), BF16),
         pltpu.VMEM((nz, nt, quarter, model), BF16),
-        pltpu.VMEM((nz, nt // CS, quarter, model), F32),
-        pltpu.VMEM((nz, nt // CS, quarter, model), BF16),
-        pltpu.VMEM((nz, nt // CS, quarter, model), BF16),
-        pltpu.VMEM((nz, quarter, model), BF16),
-        pltpu.VMEM((nz, quarter, model), BF16),
-        pltpu.VMEM((nz, quarter, model), BF16),
-        pltpu.VMEM((nz, quarter, model), BF16),
+        pltpu.VMEM((nz * rows, share), BF16),
+        pltpu.VMEM((nz, nt // CS, nz, quarter, group), F32),
+        pltpu.VMEM((nz, nt // CS, nz, quarter, group), BF16),
+        pltpu.VMEM((nz, nt // CS, nz, quarter, group), BF16),
+        pltpu.VMEM((nz, nz, quarter, group), BF16),
+        pltpu.VMEM((nz, nz, quarter, group), BF16),
+        pltpu.VMEM((nz, nz, quarter, group), BF16),
+        pltpu.VMEM((nz, nz, quarter, group), BF16),
         dma,
+        dma((2,)),
         dma((3,)),
         dma((3, nz)),
         dma((3, nz)),
@@ -589,6 +656,8 @@
         dma((2,)),
         dma((2, nz)),
         dma((2, nz)),
+        dma,
+        dma,
         dma((nt,)),
         dma((nt,)),
         dma((nz,)),
@@ -599,13 +668,13 @@
         dma((nz,)),
         dma((nz,)),
         dma((nz,)),
-        dma((nz,)),
-        dma((nz,)),
+        dma((nz, nz)),
+        dma((nz, nz)),
     ]
     return pl.pallas_call(
         functools.partial(kernel, nz, nt),
         out_shape=jax.ShapeDtypeStruct((quarter, model), BF16),
-        in_specs=[vmem] * 10 + [anyspace] * 4,
+        in_specs=[vmem] * 8 + [anyspace] * 4,
         out_specs=vmem,
         scratch_shapes=scratch,
         compiler_params=pltpu.CompilerParams(
@@ -616,16 +685,14 @@
         key_rows,
         value_rows,
         gate_input,
-        log_decay,
-        cos,
-        sin,
+        log_decay.T,
         head_gain.reshape(1, wide),
         residual,
         mlp_gain.reshape(1, model),
         out_weight,
-        gw,
-        uw,
-        dw,
+        gate_weight,
+        up_weight,
+        down_weight,
     )
 
 
@@ -641,6 +708,8 @@
         and hidden % (16 * nz) == 0
         and wide // log_decay.shape[1] == 128
         and BLOCK % (16 * nt) == 0
+        and hidden % 128 == 0
+        and log_decay.shape[1] // nt % XS == 0
     )
 
 

time: 121 us -> 110 us (0.909)
  local copies, waits for them, and re-layouts: 6.45 us -> 1.57 us
  Pallas kernels: 113 us -> 109 us
    pallas_call x1, Pallas kernels: 113 us -> 109 us  [fast_body(): pl.pallas_call(functools.partial(kernel, nz, nt), out_shape=jax.ShapeDtyp...]
    transpose x2 -> x0, local copies, waits for them, and re-layouts: 3.4 us -> none  [the longest x1 2.24 us: fast_body(): gw = gate_weight.T.reshape(nz, share, width)]
    unnamed x4 -> x1, local copies, waits for them, and re-layouts: 3.05 us -> 1.57 us
where the time goes in v2:
time: 110 us
  Pallas kernels  109 us (99%)
  local copies, waits for them, and re-layouts  1.57 us (1%)
    pallas_call x1, Pallas kernels, fast_body(): pl.pallas_call(functools.partial(kernel, nz, nt), out_shape=jax.ShapeDtyp...  109 us

profile of v2, /device:TPU:0, one launch (start us, length us, event | category | flops | bytes accessed | tf_op | source)
XLA Modules:
  0.0 110.3 jit_solution(15637055493438473507)
XLA Ops:
  0.0 108.7 %shard_map.118 = bf16[32,2048]{1,0:T(8,128)(2,1)} custom-call(bf16[128,512]{1,0:T(8,128)(2,1)} %q_ref.1, bf16[128,512]{1,0:T(8,128)(2,1)} %k_ref.1, bf16[128,512]{1,0:T(8,128)(2,1)} %v_ref.1, bf16[128,512]{1,0:T(8,128)(2,1)} %g_ref.1, f32[4,128]{1,0:T(4,128)} %bitcast.4, f32[1,512]{1,0:T(1,128)} %bitcast.5, bf16[128,2048]{1,0:T(8,128)(2,1)} %res_ref.1, ...), custom_call_target="tpu_custom_call" | custom-call | tf_op jit(solution)/shard_map/pallas_call | solution.py:674
  108.7 1.6 %copy.14 = bf16[32,2048]{1,0:T(8,128)(2,1)} copy(bf16[32,2048]{1,0:T(8,128)(2,1)} %shard_map.118) | data formatting | bytes 262144

commit v3 on v2

--- a/solution.py
+++ b/solution.py
@@ -210,6 +210,7 @@
     acc,
     norm_own,
     normed,
+    gated,
     hidden,
     keep,
     s1,
@@ -403,13 +404,11 @@
     for d in range(1, nz):
         pz[d] = go(remote(p_out, p_in.at[z], pz_send.at[0, d], pz_recv.at[0, d], z_peer(d)))
         tz[d] = go(remote(tt_out, tt_in.at[z], pz_send.at[1, d], pz_recv.at[1, d], z_peer(d)))
-    for d in [far] + near:
-        send_weight(0, d)
-    send_weight(1, far)
-    forward(0, 0)
     for d in range(1, nz):
         pz[d].wait_recv()
         tz[d].wait_recv()
+    send_weight(0, far)
+    send_weight(0, near[0])
     p_in[z] = p_out[...]
     tt_in[z] = tt_out[...]
     for i in range(hh):
@@ -423,6 +422,7 @@
         s_own[i] = jnp.where(first, state, after)
         s_out[i] = jnp.where(first, after, state).astype(BF16)
     sx = go(remote(s_out, s_in, sx_send, sx_recv, x_peer))
+    forward(0, 0)
     forward(1, 0)
     forward(2, far)
 
@@ -463,7 +463,6 @@
                     )
                 )
             )
-    forward(0, far)
     for mix in mixes:
         mix.wait_recv()
     mixed = mix_in[0].astype(F32)
@@ -477,62 +476,88 @@
         mid * lax.rsqrt(jnp.mean(mid * mid, axis=-1, keepdims=True) + EPS) * mg_ref[...]
     ).astype(BF16)
     normed[z, tp] = norm_own[...]
-    ncopy, tcopy = {}, {}
-    for d in [far] + near:
-        ncopy[d] = go(
-            remote(norm_own, normed.at[z, tp], nz_send.at[d], nz_recv.at[d], z_peer(d))
-        )
-    for e in range(1, nt):
-        tcopy[0, e] = go(
-            remote(norm_own, normed.at[z, tp], nt_send.at[0, e], nt_recv.at[0, e], t_peer(e))
-        )
-    for d in near:
-        send_weight(1, d)
-    for d in near:
-        send_weight(2, d)
-    for d in near:
-        forward(0, d)
+    tcopy = {}
+
+    def share_rows(i, zz):
+        rows_at = normed.at[zz, tp]
+        for e, peer in ((1, c_peer), (2, y_peer)):
+            tcopy[i, e] = go(
+                remote(rows_at, rows_at, nt_send.at[i, e], nt_recv.at[i, e], peer)
+            )
+
+    def pass_rows(i, zz):
+        rows_at = normed.at[zz, (1 - y) * CS + c]
+        tcopy[i, 2].wait_recv()
+        tcopy[i, 3] = go(remote(rows_at, rows_at, nt_send.at[i, 3], nt_recv.at[i, 3], c_peer))
+
+    mate = z + 1 - 2 * lax.rem(z, 2)
+    mate_peer = (mate * XS + x, tp)
+    z_far, z_last = z_from(far), lax.rem(mate + far, nz)
+    n_far = go(remote(norm_own, normed.at[z, tp], nz_send.at[0], nz_recv.at[0], z_peer(far)))
+    n_mate = go(remote(norm_own, normed.at[z, tp], nz_send.at[1], nz_recv.at[1], mate_peer))
+    share_rows(0, z)
+    forward(0, far)
+    n_far.wait_recv()
+    far_rows = normed.at[z_far, tp]
+    n_pass = go(remote(far_rows, far_rows, nz_send.at[2], nz_recv.at[2], mate_peer))
+    share_rows(1, z_far)
+    send_weight(0, near[1])
+    send_weight(1, far)
+    for m in (1, 2):
+        for d in near:
+            send_weight(m, d)
+    forward(0, near[0])
+    n_mate.wait_recv()
+    share_rows(2, mate)
+    pass_rows(0, z)
+    pass_rows(1, z_far)
+    n_pass.wait_recv()
+    share_rows(3, z_last)
+    pass_rows(2, mate)
+    forward(0, near[1])
+    pass_rows(3, z_last)
     forward(1, far)
-    for d in [far] + near:
-        ncopy[d].wait_recv()
-        zz = z_from(d)
-        for e in range(1, nt):
-            tcopy[d, e] = go(
-                remote(
-                    normed.at[zz, tp],
-                    normed.at[zz, tp],
-                    nt_send.at[d, e],
-                    nt_recv.at[d, e],
-                    t_peer(e),
-                )
-            )
-    for d in near:
-        forward(1, d)
     for d in range(nz):
         f_copies[0, d].wait_recv()
+    for key in sorted(tcopy):
+        if key[1] != 2:
+            tcopy[key].wait_recv()
+
+    ns = nz * XS
+
+    def project(m, zz):
+        block = normed[zz].reshape(rows, normed.shape[3])
+        total = dot_nt(block[:, :width], w[m, 0])
+        for s in range(1, ns):
+            total += dot_nt(block[:, s * width : (s + 1) * width], w[m, s])
+        return total
+
+    def gate_rows(zz):
+        gate = project(0, zz)
+        gated[zz] = gate / (1.0 + jnp.exp(-gate))
+
+    def up_rows(zz):
+        hidden[zz * rows : (zz + 1) * rows, :] = (gated[zz] * project(1, zz)).astype(BF16)
+
+    for zz in range(nz // 2):
+        gate_rows(zz)
+    forward(1, near[0])
+    for zz in range(nz // 2, nz):
+        gate_rows(zz)
+    forward(1, near[1])
+    for d in range(nz):
         f_copies[1, d].wait_recv()
-    for key in sorted(tcopy):
-        tcopy[key].wait_recv()
-
-    ns = nz * XS
-    for zz in range(nz):
-        block = normed[zz].reshape(rows, normed.shape[3])
-        gate = dot_nt(block[:, :width], w[0, 0])
-        up = dot_nt(block[:, :width], w[1, 0])
-        for s in range(1, ns):
-            cut = block[:, s * width : (s + 1) * width]
-            gate += dot_nt(cut, w[0, s])
-            up += dot_nt(cut, w[1, s])
-        hidden[zz * rows : (zz + 1) * rows, :] = (
-            gate / (1.0 + jnp.exp(-gate)) * up
-        ).astype(BF16)
+    for zz in range(nz // 2):
+        up_rows(zz)
+    forward(2, near[0])
+    for zz in range(nz // 2, nz):
+        up_rows(zz)
+    forward(2, near[1])
 
     t1, t2, t3 = {}, {}, {}
     low = c == 0
 
     def compute(b):
-        if b in near:
-            forward(2, b)
         f_copies[2, b].wait_recv()
         for u in range(XS):
             part = dot_nn(hidden[...], w[2, z_from(b) * XS + u])
@@ -564,14 +589,18 @@
         acc[g] = acc[g] + keep[b, y, z] + r2[b, z].astype(F32)
 
     batches = [0, far] + near
-    count = len(batches)
-    for step in range(count + 2):
-        if step < count:
-            compute(batches[step])
-        if 1 <= step < count + 1:
-            second(batches[step - 1])
-        if step >= 2:
-            third(batches[step - 2])
+    compute(0)
+    compute(far)
+    second(0)
+    second(far)
+    third(0)
+    third(far)
+    compute(near[0])
+    second(near[0])
+    compute(near[1])
+    third(near[0])
+    second(near[1])
+    third(near[1])
     for b in batches:
         for e in [far] + near:
             t3[b, e].wait_recv()
@@ -637,6 +666,7 @@
         pltpu.VMEM((nz, quarter, group), F32),
         pltpu.VMEM((quarter, model), BF16),
         pltpu.VMEM((nz, nt, quarter, model), BF16),
+        pltpu.VMEM((nz, rows, share), F32),
         pltpu.VMEM((nz * rows, share), BF16),
         pltpu.VMEM((nz, nt // CS, nz, quarter, group), F32),
         pltpu.VMEM((nz, nt // CS, nz, quarter, group), BF16),
@@ -699,7 +729,7 @@
 def fits(mesh, queries, log_decay, gate_weight):
     ns, nt = mesh.shape["sp"], mesh.shape["tp"]
     tokens, wide = queries.shape
-    if ns % XS or ns // XS < 3 or nt != 2 * CS or tokens // ns != BLOCK:
+    if ns % XS or ns // XS != 4 or nt != 2 * CS or tokens // ns != BLOCK:
         return False
     nz = ns // XS
     hidden = gate_weight.shape[1] // nt

time: 110 us -> 99.5 us (0.905)
  Pallas kernels: 109 us -> 97.8 us
    pallas_call x1, Pallas kernels: 109 us -> 97.8 us  [fast_body(): pl.pallas_call(functools.partial(kernel, nz, nt), out_shape=jax.ShapeDtyp...]
where the time goes in v3:
time: 99.5 us; the launch traced here: 99.4 us
  Pallas kernels  97.8 us (98%)
  local copies, waits for them, and re-layouts  1.57 us (2%)
    pallas_call x1, Pallas kernels, fast_body(): pl.pallas_call(functools.partial(kernel, nz, nt), out_shape=jax.ShapeDtyp...  97.8 us

profile of v3, /device:TPU:0, one launch (start us, length us, event | category | flops | bytes accessed | tf_op | source)
XLA Modules:
  0.0 99.4 jit_solution(12989761702427578341)
XLA Ops:
  0.0 97.8 %shard_map.118 = bf16[32,2048]{1,0:T(8,128)(2,1)} custom-call(bf16[128,512]{1,0:T(8,128)(2,1)} %q_ref.1, bf16[128,512]{1,0:T(8,128)(2,1)} %k_ref.1, bf16[128,512]{1,0:T(8,128)(2,1)} %v_ref.1, bf16[128,512]{1,0:T(8,128)(2,1)} %g_ref.1, f32[4,128]{1,0:T(4,128)} %bitcast.4, f32[1,512]{1,0:T(1,128)} %bitcast.5, bf16[128,2048]{1,0:T(8,128)(2,1)} %res_ref.1, ...), custom_call_target="tpu_custom_call" | custom-call | tf_op jit(solution)/shard_map/pallas_call | solution.py:704
  97.8 1.6 %copy.14 = bf16[32,2048]{1,0:T(8,128)(2,1)} copy(bf16[32,2048]{1,0:T(8,128)(2,1)} %shard_map.118) | data formatting | bytes 262144

commit v4 on v3

--- a/solution.py
+++ b/solution.py
@@ -315,6 +315,13 @@
     peers = [z_peer(d) for d in range(1, nz)] + [x_peer] + [t_peer(d) for d in range(1, nt)]
     for peer in peers:
         pl.semaphore_signal(barrier, inc=1, device_id=peer, device_id_type=MESH)
+    for m in range(2):
+        raw_copies[m].wait()
+        for j in range(raw.shape[2] // 128):
+            turned[m, j * 128 : (j + 1) * 128, :] = jnp.transpose(
+                raw[m, :, j * 128 : (j + 1) * 128]
+            )
+        take_own(m)
     pl.semaphore_wait(barrier, len(peers))
 
     w_copies = {}
@@ -338,7 +345,7 @@
 
     far = 2
     near = [d for d in range(1, nz) if d != far]
-    send_weight(2, far)
+    send_weight(1, far)
 
     ti = lax.broadcasted_iota(jnp.int32, (rows, rows), 0)
     si = lax.broadcasted_iota(jnp.int32, (rows, rows), 1)
@@ -383,14 +390,7 @@
     mine_h, other_h = x * hh, (1 - x) * hh
     cx = go(remote(c_out.at[pl.ds(other_h, hh)], c_in, cx_send.at[0], cx_recv.at[0], x_peer))
     tx = go(remote(t_out, t_in, cx_send.at[1], cx_recv.at[1], x_peer))
-    forward(2, 0)
-    for m in range(2):
-        raw_copies[m].wait()
-        for j in range(raw.shape[2] // 128):
-            turned[m, j * 128 : (j + 1) * 128, :] = jnp.transpose(
-                raw[m, :, j * 128 : (j + 1) * 128]
-            )
-        take_own(m)
+    forward(1, 0)
     cx.wait_recv()
     tx.wait_recv()
     first = x == 0
@@ -423,8 +423,7 @@
         s_out[i] = jnp.where(first, after, state).astype(BF16)
     sx = go(remote(s_out, s_in, sx_send, sx_recv, x_peer))
     forward(0, 0)
-    forward(1, 0)
-    forward(2, far)
+    forward(1, far)
 
     def finish(h, state, cols):
         cross = lax.dot_general(
@@ -471,7 +470,9 @@
     mine = pl.multiple_of(tp * quarter, quarter)
     mid = (res_ref[pl.ds(mine, quarter), :].astype(F32) + mixed).astype(BF16).astype(F32)
     for g in range(nz):
-        acc[g] = mid[:, g * group : (g + 1) * group]
+        for u in range(XS):
+            at = g * group + u * width
+            acc[g, u] = mid[:, at : at + width]
     norm_own[...] = (
         mid * lax.rsqrt(jnp.mean(mid * mid, axis=-1, keepdims=True) + EPS) * mg_ref[...]
     ).astype(BF16)
@@ -497,15 +498,16 @@
     n_mate = go(remote(norm_own, normed.at[z, tp], nz_send.at[1], nz_recv.at[1], mate_peer))
     share_rows(0, z)
     forward(0, far)
+    forward(2, 0)
     n_far.wait_recv()
     far_rows = normed.at[z_far, tp]
     n_pass = go(remote(far_rows, far_rows, nz_send.at[2], nz_recv.at[2], mate_peer))
     share_rows(1, z_far)
     send_weight(0, near[1])
-    send_weight(1, far)
-    for m in (1, 2):
-        for d in near:
-            send_weight(m, d)
+    for d in near:
+        send_weight(1, d)
+    for d in [far] + near:
+        send_weight(2, d)
     forward(0, near[0])
     n_mate.wait_recv()
     share_rows(2, mate)
@@ -516,7 +518,7 @@
     pass_rows(2, mate)
     forward(0, near[1])
     pass_rows(3, z_last)
-    forward(1, far)
+    forward(1, near[0])
     for d in range(nz):
         f_copies[0, d].wait_recv()
     for key in sorted(tcopy):
@@ -541,73 +543,98 @@
 
     for zz in range(nz // 2):
         gate_rows(zz)
-    forward(1, near[0])
+    forward(1, near[1])
     for zz in range(nz // 2, nz):
         gate_rows(zz)
-    forward(1, near[1])
+    forward(2, far)
     for d in range(nz):
         f_copies[1, d].wait_recv()
-    for zz in range(nz // 2):
+    for zz in range(nz):
         up_rows(zz)
-    forward(2, near[0])
-    for zz in range(nz // 2, nz):
-        up_rows(zz)
-    forward(2, near[1])
 
     t1, t2, t3 = {}, {}, {}
     low = c == 0
 
-    def compute(b):
-        f_copies[2, b].wait_recv()
-        for u in range(XS):
-            part = dot_nn(hidden[...], w[2, z_from(b) * XS + u])
-            cols = slice(u * width, (u + 1) * width)
-            for zz in range(nz):
-                for yy in range(nt // CS):
-                    at = zz * rows + yy * CS * quarter
-                    even = part[at : at + quarter]
-                    odd = part[at + quarter : at + 2 * quarter]
-                    keep[b, yy, zz, :, cols] = jnp.where(low, even, odd)
-                    s1[b, yy, zz, :, cols] = jnp.where(low, odd, even).astype(BF16)
-        t1[b] = go(remote(s1.at[b], r1.at[b], t1_send.at[b], t1_recv.at[b], c_peer))
-
-    def second(b):
-        t1[b].wait_recv()
-        s2[b] = (keep[b, 1 - y] + r1[b, 1 - y].astype(F32)).astype(BF16)
-        t2[b] = go(remote(s2.at[b], r2.at[b], t2_send.at[b], t2_recv.at[b], y_peer))
-        keep[b, y] = keep[b, y] + r1[b, y].astype(F32)
-
-    def third(b):
-        t2[b].wait_recv()
+    def side(u):
+        return x if u == 0 else 1 - x
+
+    def compute(b, u):
+        if u:
+            f_copies[2, b].wait_recv()
+        part = dot_nn(hidden[...], w[2, z_from(b) * XS + side(u)])
+        for zz in range(nz):
+            for yy in range(nt // CS):
+                at = zz * rows + yy * CS * quarter
+                even = part[at : at + quarter]
+                odd = part[at + quarter : at + 2 * quarter]
+                keep[b, u, yy, zz] = jnp.where(low, even, odd)
+                s1[b, u, yy, zz] = jnp.where(low, odd, even).astype(BF16)
+        t1[b, u] = go(
+            remote(s1.at[b, u], r1.at[b, u], t1_send.at[b, u], t1_recv.at[b, u], c_peer)
+        )
+
+    def second(b, u):
+        t1[b, u].wait_recv()
+        s2[b, u] = (keep[b, u, 1 - y] + r1[b, u, 1 - y].astype(F32)).astype(BF16)
+        t2[b, u] = go(
+            remote(s2.at[b, u], r2.at[b, u], t2_send.at[b, u], t2_recv.at[b, u], y_peer)
+        )
+        keep[b, u, y] = keep[b, u, y] + r1[b, u, y].astype(F32)
+
+    def third(b, u):
+        t2[b, u].wait_recv()
         for e in [far] + near:
             zz = z_at(e)
-            s3[b, e] = (keep[b, y, zz] + r2[b, zz].astype(F32)).astype(BF16)
-            t3[b, e] = go(
-                remote(s3.at[b, e], r3.at[b, e], t3_send.at[b, e], t3_recv.at[b, e], z_peer(e))
+            s3[b, u, e] = (keep[b, u, y, zz] + r2[b, u, zz].astype(F32)).astype(BF16)
+            t3[b, u, e] = go(
+                remote(
+                    s3.at[b, u, e],
+                    r3.at[b, u, e],
+                    t3_send.at[b, u, e],
+                    t3_recv.at[b, u, e],
+                    z_peer(e),
+                )
             )
-        g = z_from(b)
-        acc[g] = acc[g] + keep[b, y, z] + r2[b, z].astype(F32)
-
-    batches = [0, far] + near
-    compute(0)
-    compute(far)
-    second(0)
-    second(far)
-    third(0)
-    third(far)
-    compute(near[0])
-    second(near[0])
-    compute(near[1])
-    third(near[0])
-    second(near[1])
-    third(near[1])
-    for b in batches:
+        g, v = z_from(b), side(u)
+        acc[g, v] = acc[g, v] + keep[b, u, y, z] + r2[b, u, z].astype(F32)
+
+    n0, n1 = near
+    compute(0, 0)
+    compute(0, 1)
+    compute(far, 0)
+    second(0, 0)
+    second(0, 1)
+    forward(2, n0)
+    compute(n0, 0)
+    compute(far, 1)
+    second(far, 0)
+    forward(2, n1)
+    compute(n1, 0)
+    second(n0, 0)
+    second(far, 1)
+    third(0, 0)
+    third(0, 1)
+    second(n1, 0)
+    compute(n0, 1)
+    third(far, 0)
+    third(n0, 0)
+    second(n0, 1)
+    compute(n1, 1)
+    third(far, 1)
+    second(n1, 1)
+    third(n1, 0)
+    third(n0, 1)
+    third(n1, 1)
+    order = [(0, 0), (0, 1), (far, 0), (n0, 0), (far, 1), (n1, 0), (n0, 1), (n1, 1)]
+    for b, u in order:
         for e in [far] + near:
-            t3[b, e].wait_recv()
-            g = lax.rem(z - e - b + 2 * nz, nz)
-            acc[g] = acc[g] + r3[b, e].astype(F32)
+            t3[b, u, e].wait_recv()
+            g, v = lax.rem(z - e - b + 2 * nz, nz), side(u)
+            acc[g, v] = acc[g, v] + r3[b, u, e].astype(F32)
     for g in range(nz):
-        out_ref[:, g * group : (g + 1) * group] = acc[g].astype(BF16)
+        for u in range(XS):
+            at = g * group + u * width
+            out_ref[:, at : at + width] = acc[g, u].astype(BF16)
     for copy in started:
         copy.wait_send()
 
@@ -663,18 +690,18 @@
         pltpu.VMEM((rows, wide), BF16),
         pltpu.VMEM((nt, quarter, model), BF16),
         pltpu.VMEM((nt, quarter, model), BF16),
-        pltpu.VMEM((nz, quarter, group), F32),
+        pltpu.VMEM((nz, XS, quarter, width), F32),
         pltpu.VMEM((quarter, model), BF16),
         pltpu.VMEM((nz, nt, quarter, model), BF16),
         pltpu.VMEM((nz, rows, share), F32),
         pltpu.VMEM((nz * rows, share), BF16),
-        pltpu.VMEM((nz, nt // CS, nz, quarter, group), F32),
-        pltpu.VMEM((nz, nt // CS, nz, quarter, group), BF16),
-        pltpu.VMEM((nz, nt // CS, nz, quarter, group), BF16),
-        pltpu.VMEM((nz, nz, quarter, group), BF16),
-        pltpu.VMEM((nz, nz, quarter, group), BF16),
-        pltpu.VMEM((nz, nz, quarter, group), BF16),
-        pltpu.VMEM((nz, nz, quarter, group), BF16),
+        pltpu.VMEM((nz, XS, nt // CS, nz, quarter, width), F32),
+        pltpu.VMEM((nz, XS, nt // CS, nz, quarter, width), BF16),
+        pltpu.VMEM((nz, XS, nt // CS, nz, quarter, width), BF16),
+        pltpu.VMEM((nz, XS, nz, quarter, width), BF16),
+        pltpu.VMEM((nz, XS, nz, quarter, width), BF16),
+        pltpu.VMEM((nz, XS, nz, quarter, width), BF16),
+        pltpu.VMEM((nz, XS, nz, quarter, width), BF16),
         dma,
         dma((2,)),
         dma((3,)),
@@ -694,12 +721,12 @@
         dma((nz,)),
         dma((nz, nt)),
         dma((nz, nt)),
-        dma((nz,)),
-        dma((nz,)),
-        dma((nz,)),
-        dma((nz,)),
-        dma((nz, nz)),
-        dma((nz, nz)),
+        dma((nz, XS)),
+        dma((nz, XS)),
+        dma((nz, XS)),
+        dma((nz, XS)),
+        dma((nz, XS, nz)),
+        dma((nz, XS, nz)),
     ]
     return pl.pallas_call(
         functools.partial(kernel, nz, nt),

time: 99.5 us -> 95.8 us (0.963)
  Pallas kernels: 97.8 us -> 94 us
    pallas_call x1, Pallas kernels: 97.8 us -> 94 us  [fast_body(): pl.pallas_call(functools.partial(kernel, nz, nt), out_shape=jax.ShapeDtyp...]
where the time goes in v4:
time: 95.8 us; the launch traced here: 95.6 us
  Pallas kernels  94 us (98%)
  local copies, waits for them, and re-layouts  1.57 us (2%)
    pallas_call x1, Pallas kernels, fast_body(): pl.pallas_call(functools.partial(kernel, nz, nt), out_shape=jax.ShapeDtyp...  94 us

profile of v4, /device:TPU:0, one launch (start us, length us, event | category | flops | bytes accessed | tf_op | source)
XLA Modules:
  0.0 95.6 jit_solution(5405048690658384560)
XLA Ops:
  0.0 94.0 %shard_map.118 = bf16[32,2048]{1,0:T(8,128)(2,1)} custom-call(bf16[128,512]{1,0:T(8,128)(2,1)} %q_ref.1, bf16[128,512]{1,0:T(8,128)(2,1)} %k_ref.1, bf16[128,512]{1,0:T(8,128)(2,1)} %v_ref.1, bf16[128,512]{1,0:T(8,128)(2,1)} %g_ref.1, f32[4,128]{1,0:T(4,128)} %bitcast.4, f32[1,512]{1,0:T(1,128)} %bitcast.5, bf16[128,2048]{1,0:T(8,128)(2,1)} %res_ref.1, ...), custom_call_target="tpu_custom_call" | custom-call | tf_op jit(solution)/shard_map/pallas_call | solution.py:731
  94.1 1.6 %copy.14 = bf16[32,2048]{1,0:T(8,128)(2,1)} copy(bf16[32,2048]{1,0:T(8,128)(2,1)} %shard_map.118) | data formatting | bytes 262144

commit v5 on v4

--- a/solution.py
+++ b/solution.py
@@ -506,8 +506,6 @@
     send_weight(0, near[1])
     for d in near:
         send_weight(1, d)
-    for d in [far] + near:
-        send_weight(2, d)
     forward(0, near[0])
     n_mate.wait_recv()
     share_rows(2, mate)
@@ -517,6 +515,8 @@
     share_rows(3, z_last)
     pass_rows(2, mate)
     forward(0, near[1])
+    for d in [far] + near:
+        send_weight(2, d)
     pass_rows(3, z_last)
     forward(1, near[0])
     for d in range(nz):

time: 95.8 us -> 95.8 us (level)
  no operation moved by 1% of the time
where the time goes in v5:
time: 95.8 us; the launch traced here: 95.6 us
  Pallas kernels  94 us (98%)
  local copies, waits for them, and re-layouts  1.57 us (2%)
    pallas_call x1, Pallas kernels, fast_body(): pl.pallas_call(functools.partial(kernel, nz, nt), out_shape=jax.ShapeDtyp...  94 us

profile of v5, /device:TPU:0, one launch (start us, length us, event | category | flops | bytes accessed | tf_op | source)
XLA Modules:
  0.0 95.6 jit_solution(6832225736082929105)
XLA Ops:
  0.0 94.0 %shard_map.118 = bf16[32,2048]{1,0:T(8,128)(2,1)} custom-call(bf16[128,512]{1,0:T(8,128)(2,1)} %q_ref.1, bf16[128,512]{1,0:T(8,128)(2,1)} %k_ref.1, bf16[128,512]{1,0:T(8,128)(2,1)} %v_ref.1, bf16[128,512]{1,0:T(8,128)(2,1)} %g_ref.1, f32[4,128]{1,0:T(4,128)} %bitcast.4, f32[1,512]{1,0:T(1,128)} %bitcast.5, bf16[128,2048]{1,0:T(8,128)(2,1)} %res_ref.1, ...), custom_call_target="tpu_custom_call" | custom-call | tf_op jit(solution)/shard_map/pallas_call | solution.py:731
  94.1 1.6 %copy.14 = bf16[32,2048]{1,0:T(8,128)(2,1)} copy(bf16[32,2048]{1,0:T(8,128)(2,1)} %shard_map.118) | data formatting | bytes 262144
